TPU v7x, 32 devices: a whole 2x2x4 slice. The times are simulated.
32 devices in a mesh: sp: 8 (over z, x), tp: 4 (over y, core).
Axes of the slice: x: 2, y: 2, z: 4, core: 2. Of those that a mesh axis runs over, the one named last changes fastest.
Arguments:
- query_wide: bfloat16 [1024, 1536], P('sp', 'tp'), may hold values from -600 to 600
- query_narrow: bfloat16 [1024, 1024], P('sp', 'tp'), may hold values from -600 to 600
- latent: bfloat16 [1024, 512], P('sp'), may hold values from -6 to 6
- rope_key: bfloat16 [1024, 64], P('sp'), may hold values from -6 to 6
- latent_norm_weight: float32 [512], replicated, may hold values from 0.1 to 1.9
- broad_key_lift: bfloat16 [512, 1024], P(None, 'tp'), may hold values from -0.25 to 0.25
- broad_value_lift: bfloat16 [512, 1024], P(None, 'tp'), may hold values from -0.25 to 0.25
- slim_key_lift: bfloat16 [512, 512], P(None, 'tp'), may hold values from -0.25 to 0.25
- slim_value_lift: bfloat16 [512, 512], P(None, 'tp'), may hold values from -0.25 to 0.25
- out_wide: bfloat16 [1024, 2048], P('tp'), may hold values from -0.4375 to 0.4375
- out_narrow: bfloat16 [512, 2048], P('tp'), may hold values from -0.4375 to 0.4375
- resid: bfloat16 [1024, 2048], P('sp'), may hold values from -20 to 20
- ffn_gain: float32 [2048], replicated, may hold values from 0.1 to 1.9
- group_route: int32 [1024], P('sp'), may hold values from 0 to 7, as said below
- expert_pair: int32 [1024, 2], P('sp'), may hold values from 0 to 3, all different within a row
- group_prob: float32 [1024], P('sp'), may hold values from 0.2 to 1
- expert_prob: float32 [1024, 2], P('sp'), may hold values from 0.05 to 1
- gate_weight: bfloat16 [8, 4, 2048, 512], P('sp', None, None, 'tp'), may hold values from -0.125 to 0.125
- up_weight: bfloat16 [8, 4, 2048, 512], P('sp', None, None, 'tp'), may hold values from -0.125 to 0.125
- down_weight: bfloat16 [8, 4, 512, 2048], P('sp', None, 'tp'), may hold values from -0.25 to 0.25
Outputs:
- mixed: bfloat16 [1024, 2048], P('sp', 'tp')
Inputs may be any that keep to these rules, and one draw needn't show every extreme that they name: `group_route`: of the 128 tokens of one index of sp at most 32 name one group; in every draw one group is named by exactly 32 tokens of every index of sp, and every index of sp names one more group exactly 32 times. `expert_pair`: A token's two experts are different.
All inputs are finite; a program needn't handle non-finite values.
Results may differ from a plain program's by a relative error of at most 0.017.
Values may be sent and summed in bfloat16 or wider, within the bound.
A program may use at most 128 MiB of HBM per device.

v0:
```python
import math
import jax
import jax.numpy as jnp
from jax import lax
from jax.sharding import PartitionSpec as P

PLAIN_WIDTH_WIDE = 128
PLAIN_WIDTH_SLIM = 64
ROPE = 64
VALUE_WIDTH_WIDE = 128
VALUE_WIDTH_SLIM = 64
EPG = 4
ROPE_BASE = 10000.0
EPSILON = 1e-06
MASKED = -1e30


def rms_scale(values, gain_row):
    widened = values.astype(jnp.float32)
    return (
        widened
        * lax.rsqrt(jnp.mean(widened * widened, axis=-1, keepdims=True) + EPSILON)
        * gain_row
    )


def angles(positions, width):
    frequency = 1.0 / ROPE_BASE ** (jnp.arange(0, width, 2).astype(jnp.float32) / width)
    return positions.astype(jnp.float32)[:, None] * frequency[None, :]


def rotary(values, angle_table):
    half_width = values.shape[-1] // 2
    first_half = values[..., :half_width]
    second = values[..., half_width:]
    return jnp.concatenate(
        [
            first_half * jnp.cos(angle_table) - second * jnp.sin(angle_table),
            second * jnp.cos(angle_table) + first_half * jnp.sin(angle_table),
        ],
        axis=-1,
    )


def split_query(queries, head_count, nope_width, angle_table):
    shaped = queries.reshape(queries.shape[0], head_count, nope_width + ROPE)
    turned = rotary(shaped[..., nope_width:].astype(jnp.float32), angle_table[:, None, :]).astype(
        jnp.bfloat16
    )
    return (shaped[..., :nope_width], turned)


def group_step(
    carry_state, query_pair, key_block, value_block, rot_block, key_pos, query_pos, scale
):
    row_peak, row_total, accum_out = carry_state
    scores = jnp.einsum(
        "thd,khd->htk", query_pair[0], key_block, preferred_element_type=jnp.float32
    )
    scores = scores + jnp.einsum(
        "thd,kd->htk", query_pair[1], rot_block, preferred_element_type=jnp.float32
    )
    scores = jnp.where((query_pos[:, None] >= key_pos[None, :])[None], scores * scale, MASKED)
    new_peak = jnp.maximum(row_peak, jnp.max(scores, axis=-1))
    keep_factor = jnp.exp(row_peak - new_peak)
    weights = jnp.exp(scores - new_peak[:, :, None])
    row_total = row_total * keep_factor + jnp.sum(weights, axis=-1)
    accum_out = accum_out * keep_factor.T[:, :, None] + jnp.einsum(
        "htk,khd->thd",
        weights.astype(jnp.bfloat16),
        value_block,
        preferred_element_type=jnp.float32,
    )
    return (new_peak, row_total, accum_out)


def empty_state(head_count, width, local_tokens):
    return (
        jnp.full((head_count, local_tokens), MASKED, jnp.float32),
        jnp.zeros((head_count, local_tokens), jnp.float32),
        jnp.zeros((local_tokens, head_count, width), jnp.float32),
    )


def finish(carry_state):
    normalized = carry_state[2] / carry_state[1].T[:, :, None]
    return normalized.astype(jnp.bfloat16).reshape(normalized.shape[0], -1)


def project(latent_rows, weight):
    return jnp.dot(latent_rows, weight, preferred_element_type=jnp.float32).astype(jnp.bfloat16)


def body(
    query_wide,
    query_narrow,
    latent,
    rope_key,
    latent_norm_weight,
    broad_key_lift,
    broad_value_lift,
    slim_key_lift,
    slim_value_lift,
    out_wide,
    out_narrow,
    resid,
    ffn_gain,
    group_route,
    expert_pair,
    group_prob,
    expert_prob,
    gate_weight,
    up_weight,
    down_weight,
):
    local_tokens = latent.shape[0]
    offset = lax.axis_index("sp") * local_tokens
    query_pos = offset + jnp.arange(local_tokens, dtype=jnp.int32)
    angle_table = angles(query_pos, ROPE)
    latent_rows = rms_scale(latent, latent_norm_weight).astype(jnp.bfloat16)
    rot_key = rotary(rope_key.astype(jnp.float32), angle_table).astype(jnp.bfloat16)
    heads_wide = query_wide.shape[1] // (PLAIN_WIDTH_WIDE + ROPE)
    heads_narrow = query_narrow.shape[1] // (PLAIN_WIDTH_SLIM + ROPE)
    wide_query = split_query(query_wide, heads_wide, PLAIN_WIDTH_WIDE, angle_table)
    narrow_query = split_query(query_narrow, heads_narrow, PLAIN_WIDTH_SLIM, angle_table)

    def expand(lat_block):
        return (
            project(lat_block, broad_key_lift),
            project(lat_block, broad_value_lift),
            project(lat_block, slim_key_lift),
            project(lat_block, slim_value_lift),
        )

    def attend(carry_state, key_set, key_pos):
        key_w, value_w, key_n, value_n, rot_block = key_set
        block_rows = rot_block.shape[0]
        wide_state = group_step(
            carry_state[0],
            wide_query,
            key_w.reshape(block_rows, heads_wide, PLAIN_WIDTH_WIDE),
            value_w.reshape(block_rows, heads_wide, VALUE_WIDTH_WIDE),
            rot_block,
            key_pos,
            query_pos,
            (PLAIN_WIDTH_WIDE + ROPE) ** (-0.5),
        )
        narrow_state = group_step(
            carry_state[1],
            narrow_query,
            key_n.reshape(block_rows, heads_narrow, PLAIN_WIDTH_SLIM),
            value_n.reshape(block_rows, heads_narrow, VALUE_WIDTH_SLIM),
            rot_block,
            key_pos,
            query_pos,
            (PLAIN_WIDTH_SLIM + ROPE) ** (-0.5),
        )
        return (wide_state, narrow_state)

    start_state = (
        empty_state(heads_wide, VALUE_WIDTH_WIDE, local_tokens),
        empty_state(heads_narrow, VALUE_WIDTH_SLIM, local_tokens),
    )
    pieces = (
        lax.all_gather(latent_rows, "sp", axis=0, tiled=True),
        lax.all_gather(rot_key, "sp", axis=0, tiled=True),
    )
    total_rows = pieces[0].shape[0]
    block_rows = math.gcd(total_rows, 1024)

    def visit_block(block_index, carry_inner):
        block_start = block_index * block_rows
        sliced = tuple(
            (lax.dynamic_slice_in_dim(piece, block_start, block_rows, 0) for piece in pieces)
        )
        key_pos = block_start + jnp.arange(block_rows, dtype=jnp.int32)

        def work_block(running):
            key_set = expand(sliced[0]) + (sliced[1],)
            return attend(running, key_set, key_pos)

        return lax.cond(
            block_start > query_pos[-1], lambda unchanged: unchanged, work_block, carry_inner
        )

    final_state = lax.fori_loop(0, total_rows // block_rows, visit_block, start_state)
    att_wide = finish(final_state[0])
    att_narrow = finish(final_state[1])
    partial_value = jnp.dot(att_wide, out_wide, preferred_element_type=jnp.float32)
    partial_value = partial_value + jnp.dot(
        att_narrow, out_narrow, preferred_element_type=jnp.float32
    )
    model_width = resid.shape[1]
    tp_size = lax.axis_size("tp")
    quarter = model_width // tp_size
    col_start = lax.axis_index("tp") * quarter
    summed = lax.psum(partial_value.astype(jnp.bfloat16), "tp").astype(jnp.float32)
    stream = (resid.astype(jnp.float32) + summed).astype(jnp.bfloat16)
    normed = rms_scale(stream, ffn_gain).astype(jnp.bfloat16)
    stream_cols = lax.dynamic_slice_in_dim(stream, col_start, quarter, 1)
    groups = lax.axis_size("sp")
    capacity = 2 * local_tokens // groups
    share_of = group_prob[:, None] * expert_prob / jnp.sum(expert_prob, axis=1, keepdims=True)
    chosen = (expert_pair[:, :, None] == jnp.arange(EPG, dtype=jnp.int32)[None, None, :]).astype(
        jnp.float32
    )
    combine = jnp.sum(share_of[:, :, None] * chosen, axis=1).astype(jnp.bfloat16)
    member = (group_route[:, None] == jnp.arange(groups, dtype=jnp.int32)[None, :]).astype(
        jnp.int32
    )
    group_rank = jnp.sum(jnp.cumsum(member, axis=0) * member, axis=1) - 1
    slot_index = group_route * capacity + group_rank
    routed_weights = jnp.zeros((groups * capacity, EPG), jnp.bfloat16).at[slot_index].set(combine)
    routed_weights = routed_weights.reshape(groups, capacity, EPG)
    column_rows = lax.dynamic_slice_in_dim(normed, col_start, quarter, 1)
    placed = (
        jnp.zeros((groups * capacity, column_rows.shape[1]), jnp.bfloat16)
        .at[slot_index]
        .set(column_rows)
    )
    joined = lax.all_gather(
        lax.all_to_all(
            placed.reshape(groups, capacity, column_rows.shape[1]),
            "sp",
            split_axis=0,
            concat_axis=0,
            tiled=True,
        ),
        "tp",
        axis=2,
        tiled=True,
    )
    slot_count = joined.shape[0] * joined.shape[1]
    flat_rows = joined.reshape(slot_count, joined.shape[2])
    gate_act = jnp.einsum(
        "rd,edf->ref", flat_rows, gate_weight[0], preferred_element_type=jnp.float32
    )
    up_act = jnp.einsum("rd,edf->ref", flat_rows, up_weight[0], preferred_element_type=jnp.float32)
    scaled = (
        lax.all_to_all(routed_weights, "sp", split_axis=0, concat_axis=0, tiled=True)
        .reshape(slot_count, EPG)
        .astype(jnp.float32)[:, :, None]
    )
    hidden = (jax.nn.silu(gate_act) * up_act * scaled).astype(jnp.bfloat16)
    partials = jnp.einsum("ref,efd->rd", hidden, down_weight[0], preferred_element_type=jnp.float32)
    partials = partials.reshape(joined.shape)
    summed_rows = lax.psum_scatter(
        partials.astype(jnp.bfloat16), "tp", scatter_dimension=2, tiled=True
    )
    returned_rows = lax.all_to_all(summed_rows, "sp", split_axis=0, concat_axis=0, tiled=True)
    moe_rows = returned_rows.reshape(groups * capacity, quarter)[slot_index]
    return (stream_cols.astype(jnp.float32) + moe_rows.astype(jnp.float32)).astype(jnp.bfloat16)


def solution(mesh):
    placed = (
        P("sp", "tp"),
        P("sp", "tp"),
        P("sp", None),
        P("sp", None),
        P(),
        P(None, "tp"),
        P(None, "tp"),
        P(None, "tp"),
        P(None, "tp"),
        P("tp", None),
        P("tp", None),
        P("sp", None),
        P(),
        P("sp"),
        P("sp", None),
        P("sp"),
        P("sp", None),
        P("sp", None, None, "tp"),
        P("sp", None, None, "tp"),
        P("sp", None, "tp", None),
    )
    return jax.shard_map(body, mesh=mesh, in_specs=placed, out_specs=P("sp", "tp"), check_vma=False)
```

profile of v0, /device:TPU:0, one launch (start us, length us, event | category | flops | bytes accessed | tf_op | source)
XLA Modules:
  0.0 180.7 jit_solution(8999266724435186518)
XLA Ops:
  6.5 1.2 fusion.38
  7.7 1.7 fusion.40
  10.2 1.0 copy.74
  11.2 1.0 copy.75
  14.6 28.3 %all_gather.10 = bf16[1024,64]{0,1:T(8,128)(2,1)S(1)} all-gather(bf16[128,64]{0,1:T(8,128)(2,1)S(1)} %pad_maximum_fusion.2), channel_id=1, replica_groups=mesh['sp'=8,'tp'=4] {'sp'}, dimensions={0}, use_global_device_ids=true | all-gather | bytes 147456 | tf_op jit(solution)/shard_map/all_gather | solution.py:166
  43.6 9.6 %all-gather.3.cloned.1.call-done = bf16[1024,512]{1,0:T(8,128)(2,1)} async-done(((bf16[128,512]{1,0:T(8,128)(2,1)}), bf16[1024,512]{1,0:T(8,128)(2,1)}) %all-gather.3.cloned.1.call-update) | async-done | bytes 1048592 | tf_op jit(solution)/shard_map/all_gather | solution.py:165
  53.2 7.1 %conditional.1 = (f32[2,128]{1,0:T(2,128)S(1)}, f32[128,2,128]{0,2,1:T(8,128)S(1)}, f32[2,128]{1,0:T(2,128)S(1)}, f32[128,2,64]{0,2,1:T(8,128)S(1)}) conditional(s32[]{:T(128)} %bitcast.13, (s32[128]{0:T(128)S(1)}, s32[1024]{0:T(1024)S(1)}, bf16[1024,512]{1,0:T(8,128)(2,1)}, bf16[512,256]{1,0:T(8,128)(2,1)S(1)}, bf16[128,2,192]{0,2,1:T(8,128)(2,1)S(1)}, ...), branch_computations={%region_1.6_spmd, %region_6.7_spmd} | conditional | flops 1078953472 | bytes 26996452 | solution.py:182
  53.8 1.7 convolution_convert_fusion.1
  60.4 1.6 fusion.54
  62.0 1.1 fusion.23
  64.2 31.1 %all-reduce.2.cloned.1.call-done = bf16[128,2048]{1,0:T(8,128)(2,1)} async-done(((bf16[128,2048]{1,0:T(8,128)(2,1)}), bf16[128,2048]{1,0:T(8,128)(2,1)}) %all-reduce.2.cloned.1.call-update) | async-done | bytes 524304 | tf_op jit(solution)/shard_map/psum | solution.py:197
  95.3 1.3 multiply_reduce_fusion
  96.6 1.1 convert_element_type.142
  97.7 1.6 scatter_custom_fusion
  99.3 13.6 %all_to_all.15 = bf16[8,32,512]{2,1,0:T(8,128)(2,1)} all-to-all(bf16[8,32,512]{2,1,0:T(8,128)(2,1)S(1)} %bitcast.107), channel_id=1, replica_groups=mesh['sp'=8,'tp'=4] {'sp'}, dimensions={0} | all-to-all | bytes 524288 | tf_op jit(solution)/shard_map/all_to_all | solution.py:222
  113.2 0.9 scatter_custom_fusion.1
  114.2 9.7 %all_to_all.16 = bf16[8,32,4]{1,2,0:T(4,128)(2,1)S(1)} all-to-all(bf16[8,32,4]{1,2,0:T(4,128)(2,1)S(1)} %copy.78), channel_id=1, replica_groups=mesh['sp'=8,'tp'=4] {'sp'}, dimensions={0} | all-to-all | bytes 4096 | tf_op jit(solution)/shard_map/all_to_all | solution.py:240
  124.0 4.1 %all-gather.5.cloned.1.call-done = bf16[8,32,2048]{2,1,0:T(8,128)(2,1)} async-done(((bf16[8,32,512]{2,1,0:T(8,128)(2,1)}), bf16[8,32,2048]{2,1,0:T(8,128)(2,1)}) %all-gather.5.cloned.1.call-update) | async-done | bytes 1048592 | tf_op jit(solution)/shard_map/all_gather | solution.py:221
  128.1 2.8 %fusion.27 = f32[256,4,128]{2,0,1:T(8,128)S(1)} fusion(bf16[256,2048,1]{1,0,2:T(8,128)(2,1)} %bitcast.119, bf16[1,4,2048,128]{3,2,1,0:T(8,128)(2,1)} %param.39), kind=kOutput, calls=%fused_computation.49 | convolution fusion | flops 536870912 | bytes 3670016 | tf_op jit(solution)/shard_map/rd,edf->ref/dot_general | solution.py:235
  131.7 1.7 fusion.22
  133.4 24.9 %reduce-scatter.2.cloned.1.call-done = bf16[8,32,512]{2,1,0:T(8,128)(2,1)} async-done(((bf16[8,32,2048]{2,1,0:T(8,128)(2,1)}), bf16[8,32,512]{2,1,0:T(8,128)(2,1)}) %reduce-scatter.2.cloned.1.call-update) | async-done | bytes 262160 | tf_op jit(solution)/shard_map/reduce_scatter | solution.py:247
  158.3 5.5 %all-to-all-start.2 = ((bf16[8,32,512]{2,1,0:T(8,128)(2,1)}), bf16[8,32,512]{2,1,0:T(8,128)(2,1)S(1)}, u32[]{:S(2)}, u32[]{:S(2)}) async-start(bf16[8,32,512]{2,1,0:T(8,128)(2,1)} %reduce-scatter.2.cloned.1.call-done), calls=%async_computation.3 | async-start | bytes 524288 | tf_op jit(solution)/shard_map/all_to_all | solution.py:250
  163.9 8.7 %all-to-all-done.2 = bf16[8,32,512]{2,1,0:T(8,128)(2,1)S(1)} async-done(((bf16[8,32,512]{2,1,0:T(8,128)(2,1)}), bf16[8,32,512]{2,1,0:T(8,128)(2,1)S(1)}, u32[]{:S(2)}, u32[]{:S(2)}) %all-to-all-start.2) | async-done | bytes 262176 | tf_op jit(solution)/shard_map/all_to_all | solution.py:250
  172.6 0.8 gather_fusion
  (91 shorter events, 11.4 us)
Async XLA Ops:
  6.5 125.1 %copy-start = (bf16[1,4,128,2048]{3,2,1,0:T(8,128)(2,1)S(1)}, bf16[1,4,128,2048]{3,2,1,0:T(8,128)(2,1)}, u32[]{:S(2)}) copy-start(bf16[1,4,128,2048]{3,2,1,0:T(8,128)(2,1)} %param.41) | copy-start | bytes 6291460
  6.5 46.6 %copy-start.4 = (bf16[512,256]{1,0:T(8,128)(2,1)S(1)}, bf16[512,256]{1,0:T(8,128)(2,1)}, u32[]{:S(2)}) copy-start(bf16[512,256]{1,0:T(8,128)(2,1)} %param.27) | copy-start | bytes 786436
  6.5 46.6 %all-gather.3.cloned.1.call-start = ((), (), s32[]{:S(2)}) async-start(), calls=%async_computation.4 | async-start | bytes 1179648 | tf_op jit(solution)/shard_map/all_gather | solution.py:165
  9.4 85.8 %all-reduce.2.cloned.1.call-start = ((), (), s32[]{:S(2)}) async-start(), calls=%async_computation.5 | async-start | bytes 1048576 | tf_op jit(solution)/shard_map/psum | solution.py:197
  53.2 0.6 copy-start.6
  55.6 1.2 copy-start.1
  55.6 1.2 copy-start.9
  56.0 1.3 copy-start.7
  56.2 1.5 copy-start.8
  57.7 0.9 copy-start.10
  58.1 1.3 copy-start.5
  60.3 1.7 copy-start.3
  60.4 2.9 %copy-start.12 = (s32[128]{0:T(128)S(1)}, s32[128]{0:T(128)}, u32[]{:S(2)}) copy-start(s32[128]{0:T(128)} %param.35) | copy-start | bytes 1540
  60.4 34.9 %copy-start.2 = (bf16[128,2048]{1,0:T(8,128)(2,1)S(1)}, bf16[128,2048]{1,0:T(8,128)(2,1)}, u32[]{:S(2)}) copy-start(bf16[128,2048]{1,0:T(8,128)(2,1)} %param.33) | copy-start | bytes 1572868
  63.2 64.9 %all-gather.5.cloned.1.call-start = ((), (), s32[]{:S(2)}) async-start(), calls=%async_computation.6 | async-start | bytes 1310720 | tf_op jit(solution)/shard_map/all_gather | solution.py:221
  64.2 48.8 %copy-start.11 = (f32[128,2]{0,1:T(2,128)S(1)}, f32[128,2]{0,1:T(2,128)}, u32[]{:S(2)}) copy-start(f32[128,2]{0,1:T(2,128)} %param.38) | copy-start | bytes 3076
  64.2 48.8 %copy-start.14 = (f32[128]{0:T(128)S(1)}, f32[128]{0:T(128)}, u32[]{:S(2)}) copy-start(f32[128]{0:T(128)} %param.37) | copy-start | bytes 1540
  64.2 48.9 %copy-start.13 = (s32[128,2]{0,1:T(2,128)S(1)}, s32[128,2]{0,1:T(2,128)}, u32[]{:S(2)}) copy-start(s32[128,2]{0,1:T(2,128)} %param.36) | copy-start | bytes 3076
  112.9 45.4 %reduce-scatter.2.cloned.1.call-start = ((), (), s32[]{:S(2)}) async-start(), calls=%async_computation.7 | async-start | bytes 1310720 | tf_op jit(solution)/shard_map/reduce_scatter | solution.py:247
  128.1 2.8 %copy-start.15 = (bf16[1,4,2048,128]{3,2,1,0:T(8,128)(2,1)S(1)}, bf16[1,4,2048,128]{3,2,1,0:T(8,128)(2,1)}, u32[]{:S(2)}) copy-start(bf16[1,4,2048,128]{3,2,1,0:T(8,128)(2,1)} %param.40) | copy-start | bytes 6291460
  128.1 2.8 %copy-start.16 = (bf16[8,32,2048]{2,1,0:T(8,128)(2,1)S(1)}, bf16[8,32,2048]{2,1,0:T(8,128)(2,1)}, u32[]{:S(2)}) copy-start(bf16[8,32,2048]{2,1,0:T(8,128)(2,1)} %all-gather.5.cloned.1.call-done) | copy-start | bytes 3145732
  158.3 14.3 %all-to-all-start.2 = ((bf16[8,32,512]{2,1,0:T(8,128)(2,1)}), bf16[8,32,512]{2,1,0:T(8,128)(2,1)S(1)}, u32[]{:S(2)}, u32[]{:S(2)}) async-start(bf16[8,32,512]{2,1,0:T(8,128)(2,1)} %reduce-scatter.2.cloned.1.call-done), calls=%async_computation.3 | async-start | bytes 524288 | tf_op jit(solution)/shard_map/all_to_all | solution.py:250
Sparse Core Ops, SparseCore 0:
  9.5 43.5 all-gather.2
  63.3 31.9 all-reduce.1
  113.1 14.9 all-gather.4
  133.5 24.7 reduce-scatter.1
where the time goes:
time: 181 us
  waiting for transfers between devices  78.5 us (43%)
  blocking collectives  51.6 us (29%)
  between operations  14 us (8%)
  matrix products  13.2 us (7%)
  other arithmetic  10.8 us (6%)
  local copies, waits for them, and re-layouts  6.7 us (4%)
  starting transfers between devices  5.64 us (3%)
    psum x1, waiting for transfers between devices, body(): lax.psum(partial_value.astype(jnp.bfloat16), 'tp').astype(jnp.float32)  31.1 us
    all_gather x1, blocking collectives, body(): lax.all_gather(rot_key, 'sp', axis=0, tiled=True)  28.3 us
    reduce_scatter x1, waiting for transfers between devices, body(): lax.psum_scatter(partials.astype(jnp.bfloat16), 'tp', scatter_dimension=2...  24.9 us
    all_to_all x1, blocking collectives, body(): lax.all_to_all(placed.reshape(groups, capacity, column_rows.shape[1]), 's...  13.6 us
    all_to_all x1, blocking collectives, body(): lax.all_to_all(routed_weights, 'sp', split_axis=0, concat_axis=0, tiled=T...  9.66 us
    all_gather x1, waiting for transfers between devices, body(): lax.all_gather(latent_rows, 'sp', axis=0, tiled=True)  9.58 us
    all_to_all x1, waiting for transfers between devices, body(): lax.all_to_all(summed_rows, 'sp', split_axis=0, concat_axis=0, tiled=True)  8.74 us
    all_to_all x1, starting transfers between devices, body(): lax.all_to_all(summed_rows, 'sp', split_axis=0, concat_axis=0, tiled=True)  5.51 us
  transfers between devices with their start and end apart: 5, of which 5 were waited for; matrix products, arithmetic and copies ran while one was open for 4% of the time, Pallas kernels for 0%

commit v1 on v0

--- a/solution.py
+++ b/solution.py
@@ -13,6 +13,9 @@
 ROPE_BASE = 10000.0
 EPSILON = 1e-06
 MASKED = -1e30
+prepare_target = lambda patch, axis_name: jnp.sum(
+    lax.all_gather(patch, axis_name=axis_name), axis=0
+)
 
 
 def rms_scale(values, gain_row):
@@ -194,7 +197,7 @@
     tp_size = lax.axis_size("tp")
     quarter = model_width // tp_size
     col_start = lax.axis_index("tp") * quarter
-    summed = lax.psum(partial_value.astype(jnp.bfloat16), "tp").astype(jnp.float32)
+    summed = prepare_target(partial_value.astype(jnp.bfloat16), "tp").astype(jnp.float32)
     stream = (resid.astype(jnp.float32) + summed).astype(jnp.bfloat16)
     normed = rms_scale(stream, ffn_gain).astype(jnp.bfloat16)
     stream_cols = lax.dynamic_slice_in_dim(stream, col_start, quarter, 1)

time: 181 us -> 173 us (0.956)
  waiting for transfers between devices: 78.5 us -> 68.3 us
    psum x1 -> x0, waiting for transfers between devices: 31.1 us -> none  [body(): lax.psum(partial_value.astype(jnp.bfloat16), 'tp').astype(jnp.float32)]
    all_gather x0 -> x1, waiting for transfers between devices: none -> 20.2 us  [lax.all_gather(patch, axis_name=axis_name)]
    reduce_sum x0 -> x1, other arithmetic: none -> 2.02 us  [jnp.sum(lax.all_gather(patch, axis_name=axis_name), axis=0)]
where the time goes in v1:
time: 173 us; the launch traced here: 172 us
  waiting for transfers between devices  68.3 us (39%)
  blocking collectives  53 us (31%)
  between operations  14.1 us (8%)
  matrix products  13.3 us (8%)
  other arithmetic  11.6 us (7%)
  local copies, waits for them, and re-layouts  6.09 us (4%)
  starting transfers between devices  5.63 us (3%)
    all_gather x1, blocking collectives, body(): lax.all_gather(rot_key, 'sp', axis=0, tiled=True)  28.3 us
    reduce_scatter x1, waiting for transfers between devices, body(): lax.psum_scatter(partials.astype(jnp.bfloat16), 'tp', scatter_dimension=2...  24.9 us
    all_gather x1, waiting for transfers between devices, lax.all_gather(patch, axis_name=axis_name)  20.2 us
    all_to_all x1, blocking collectives, body(): lax.all_to_all(placed.reshape(groups, capacity, column_rows.shape[1]), 's...  14.7 us
    all_gather x1, waiting for transfers between devices, body(): lax.all_gather(latent_rows, 'sp', axis=0, tiled=True)  10.7 us
    all_to_all x1, blocking collectives, body(): lax.all_to_all(routed_weights, 'sp', split_axis=0, concat_axis=0, tiled=T...  9.92 us
    all_to_all x1, waiting for transfers between devices, body(): lax.all_to_all(summed_rows, 'sp', split_axis=0, concat_axis=0, tiled=True)  8.74 us
    all_to_all x1, starting transfers between devices, body(): lax.all_to_all(summed_rows, 'sp', split_axis=0, concat_axis=0, tiled=True)  5.51 us
  transfers between devices with their start and end apart: 5, of which 5 were waited for; matrix products, arithmetic and copies ran while one was open for 4% of the time, Pallas kernels for 0%

profile of v1, /device:TPU:0, one launch (start us, length us, event | category | flops | bytes accessed | tf_op | source)
XLA Modules:
  0.0 172.1 jit_solution(8464355583354757501)
XLA Ops:
  6.5 1.2 fusion.38
  7.7 1.7 fusion.40
  10.2 1.0 copy.74
  11.2 1.0 copy.75
  13.8 28.3 %all_gather.16 = bf16[1024,64]{0,1:T(8,128)(2,1)S(1)} all-gather(bf16[128,64]{0,1:T(8,128)(2,1)S(1)} %pad_maximum_fusion.2), channel_id=1, replica_groups=mesh['sp'=8,'tp'=4] {'sp'}, dimensions={0}, use_global_device_ids=true | all-gather | bytes 147456 | tf_op jit(solution)/shard_map/all_gather | solution.py:169
  42.2 10.7 %all-gather.5.cloned.1.call-done = bf16[1024,512]{1,0:T(8,128)(2,1)} async-done(((bf16[128,512]{1,0:T(8,128)(2,1)}), bf16[1024,512]{1,0:T(8,128)(2,1)}) %all-gather.5.cloned.1.call-update) | async-done | bytes 1048592 | tf_op jit(solution)/shard_map/all_gather | solution.py:168
  52.9 6.5 %conditional.1 = (f32[2,128]{1,0:T(2,128)S(1)}, f32[128,2,128]{0,2,1:T(8,128)S(1)}, f32[2,128]{1,0:T(2,128)S(1)}, f32[128,2,64]{0,2,1:T(8,128)S(1)}) conditional(s32[]{:T(128)} %bitcast.13, (s32[128]{0:T(128)S(1)}, s32[1024]{0:T(1024)S(1)}, bf16[1024,512]{1,0:T(8,128)(2,1)}, bf16[512,256]{1,0:T(8,128)(2,1)}, bf16[128,2,192]{0,2,1:T(8,128)(2,1)S(1)}, ...), branch_computations={%region_1.6_spmd, %region_6.7_spmd} | conditional | flops 1078953472 | bytes 26341008 | solution.py:185
  52.9 1.7 %convolution_convert_fusion.1 = bf16[1024,256]{0,1:T(8,128)(2,1)S(1)} fusion(bf16[1024,512]{1,0:T(8,128)(2,1)} %get-tuple-element.176, bf16[512,256]{1,0:T(8,128)(2,1)} %get-tuple-element.203), kind=kOutput, calls=%fused_computation.14 | convolution fusion | flops 268697600 | bytes 1835008 | tf_op jit(solution)/shard_map/while/body/eval_jaxpr/cond/branch_0_fun/dot_general | solution.py:94
  59.5 1.6 fusion.54
  61.1 1.1 fusion.23
  63.5 20.2 %all-gather.9.cloned.1.call-done = bf16[512,2048]{1,0:T(8,128)(2,1)} async-done(((bf16[128,2048]{1,0:T(8,128)(2,1)}), bf16[512,2048]{1,0:T(8,128)(2,1)}) %all-gather.9.cloned.1.call-update) | async-done | bytes 2097168 | tf_op jit(solution)/shard_map/all_gather | solution.py:17
  83.7 2.0 %reduce_sum.80 = bf16[128,2048]{1,0:T(8,128)(2,1)S(1)} reduce(bf16[4,128,2048]{2,1,0:T(8,128)(2,1)} %bitcast.107, bf16[]{:T(256)} %constant.81.clone.1), dimensions={0}, to_apply=%region_7.0 | reduce | flops 786432 | bytes 2621442 | tf_op jit(solution)/shard_map/reduce_sum | solution.py:16
  85.7 1.3 multiply_reduce_fusion
  87.1 1.1 convert_element_type.144
  88.2 1.6 scatter_custom_fusion
  89.8 14.7 %all_to_all.15 = bf16[8,32,512]{2,1,0:T(8,128)(2,1)} all-to-all(bf16[8,32,512]{2,1,0:T(8,128)(2,1)S(1)} %bitcast.109), channel_id=1, replica_groups=mesh['sp'=8,'tp'=4] {'sp'}, dimensions={0} | all-to-all | bytes 524288 | tf_op jit(solution)/shard_map/all_to_all | solution.py:225
  104.8 0.9 scatter_custom_fusion.1
  105.8 9.9 %all_to_all.16 = bf16[8,32,4]{1,2,0:T(4,128)(2,1)S(1)} all-to-all(bf16[8,32,4]{1,2,0:T(4,128)(2,1)S(1)} %copy.78), channel_id=1, replica_groups=mesh['sp'=8,'tp'=4] {'sp'}, dimensions={0} | all-to-all | bytes 4096 | tf_op jit(solution)/shard_map/all_to_all | solution.py:243
  115.8 3.6 %all-gather.7.cloned.1.call-done = bf16[8,32,2048]{2,1,0:T(8,128)(2,1)} async-done(((bf16[8,32,512]{2,1,0:T(8,128)(2,1)}), bf16[8,32,2048]{2,1,0:T(8,128)(2,1)}) %all-gather.7.cloned.1.call-update) | async-done | bytes 1048592 | tf_op jit(solution)/shard_map/all_gather | solution.py:224
  119.5 2.8 %fusion.27 = f32[256,4,128]{2,0,1:T(8,128)S(1)} fusion(bf16[256,2048,1]{1,0,2:T(8,128)(2,1)} %bitcast.121, bf16[1,4,2048,128]{3,2,1,0:T(8,128)(2,1)} %param.39), kind=kOutput, calls=%fused_computation.49 | convolution fusion | flops 536870912 | bytes 3670016 | tf_op jit(solution)/shard_map/rd,edf->ref/dot_general | solution.py:238
  123.0 1.7 %fusion.22 = bf16[8,32,2048]{2,1,0:T(8,128)(2,1)} fusion(bf16[8,32,4,128]{3,1,0,2:T(8,128)(2,1)S(1)} %bitcast.123, bf16[1,4,128,2048]{3,2,1,0:T(8,128)(2,1)S(1)} %copy-done), kind=kOutput, calls=%fused_computation.43 | convolution fusion | flops 537395200 | bytes 3407872 | tf_op jit(solution)/shard_map/ref,efd->rd/dot_general | solution.py:248
  124.8 24.9 %reduce-scatter.2.cloned.1.call-done = bf16[8,32,512]{2,1,0:T(8,128)(2,1)} async-done(((bf16[8,32,2048]{2,1,0:T(8,128)(2,1)}), bf16[8,32,512]{2,1,0:T(8,128)(2,1)}) %reduce-scatter.2.cloned.1.call-update) | async-done | bytes 262160 | tf_op jit(solution)/shard_map/reduce_scatter | solution.py:250
  149.7 5.5 %all-to-all-start.2 = ((bf16[8,32,512]{2,1,0:T(8,128)(2,1)}), bf16[8,32,512]{2,1,0:T(8,128)(2,1)S(1)}, u32[]{:S(2)}, u32[]{:S(2)}) async-start(bf16[8,32,512]{2,1,0:T(8,128)(2,1)} %reduce-scatter.2.cloned.1.call-done), calls=%async_computation.3 | async-start | bytes 524288 | tf_op jit(solution)/shard_map/all_to_all | solution.py:253
  155.2 8.7 %all-to-all-done.2 = bf16[8,32,512]{2,1,0:T(8,128)(2,1)S(1)} async-done(((bf16[8,32,512]{2,1,0:T(8,128)(2,1)}), bf16[8,32,512]{2,1,0:T(8,128)(2,1)S(1)}, u32[]{:S(2)}, u32[]{:S(2)}) %all-to-all-start.2) | async-done | bytes 262176 | tf_op jit(solution)/shard_map/all_to_all | solution.py:253
  (82 shorter events, 10.4 us)
Async XLA Ops:
  6.5 116.5 %copy-start = (bf16[1,4,128,2048]{3,2,1,0:T(8,128)(2,1)S(1)}, bf16[1,4,128,2048]{3,2,1,0:T(8,128)(2,1)}, u32[]{:S(2)}) copy-start(bf16[1,4,128,2048]{3,2,1,0:T(8,128)(2,1)} %param.41) | copy-start | bytes 6291460
  6.5 46.4 %all-gather.5.cloned.1.call-start = ((), (), s32[]{:S(2)}) async-start(), calls=%async_computation.4 | async-start | bytes 1179648 | tf_op jit(solution)/shard_map/all_gather | solution.py:168
  9.4 74.3 %all-gather.9.cloned.1.call-start = ((), (), s32[]{:S(2)}) async-start(), calls=%async_computation.7 | async-start | bytes 2621440 | tf_op jit(solution)/shard_map/all_gather | solution.py:17
  54.8 1.2 copy-start.1
  54.8 1.2 copy-start.4
  56.8 0.9 copy-start.5
  57.2 1.3 copy-start.3
  59.4 1.7 copy-start.2
  59.5 2.8 %copy-start.7 = (s32[128]{0:T(128)S(1)}, s32[128]{0:T(128)}, u32[]{:S(2)}) copy-start(s32[128]{0:T(128)} %param.35) | copy-start | bytes 1540
  62.2 57.2 %all-gather.7.cloned.1.call-start = ((), (), s32[]{:S(2)}) async-start(), calls=%async_computation.5 | async-start | bytes 1310720 | tf_op jit(solution)/shard_map/all_gather | solution.py:224
  85.7 18.9 %copy-start.6 = (f32[128,2]{0,1:T(2,128)S(1)}, f32[128,2]{0,1:T(2,128)}, u32[]{:S(2)}) copy-start(f32[128,2]{0,1:T(2,128)} %param.38) | copy-start | bytes 3076
  85.7 18.9 %copy-start.9 = (f32[128]{0:T(128)S(1)}, f32[128]{0:T(128)}, u32[]{:S(2)}) copy-start(f32[128]{0:T(128)} %param.37) | copy-start | bytes 1540
  85.7 18.9 %copy-start.8 = (s32[128,2]{0,1:T(2,128)S(1)}, s32[128,2]{0,1:T(2,128)}, u32[]{:S(2)}) copy-start(s32[128,2]{0,1:T(2,128)} %param.36) | copy-start | bytes 3076
  104.5 45.2 %reduce-scatter.2.cloned.1.call-start = ((), (), s32[]{:S(2)}) async-start(), calls=%async_computation.6 | async-start | bytes 1310720 | tf_op jit(solution)/shard_map/reduce_scatter | solution.py:250
  119.5 2.8 %copy-start.10 = (bf16[1,4,2048,128]{3,2,1,0:T(8,128)(2,1)S(1)}, bf16[1,4,2048,128]{3,2,1,0:T(8,128)(2,1)}, u32[]{:S(2)}) copy-start(bf16[1,4,2048,128]{3,2,1,0:T(8,128)(2,1)} %param.40) | copy-start | bytes 6291460
  119.5 2.8 %copy-start.11 = (bf16[8,32,2048]{2,1,0:T(8,128)(2,1)S(1)}, bf16[8,32,2048]{2,1,0:T(8,128)(2,1)}, u32[]{:S(2)}) copy-start(bf16[8,32,2048]{2,1,0:T(8,128)(2,1)} %all-gather.7.cloned.1.call-done) | copy-start | bytes 3145732
  149.7 14.3 %all-to-all-start.2 = ((bf16[8,32,512]{2,1,0:T(8,128)(2,1)}), bf16[8,32,512]{2,1,0:T(8,128)(2,1)S(1)}, u32[]{:S(2)}, u32[]{:S(2)}) async-start(bf16[8,32,512]{2,1,0:T(8,128)(2,1)} %reduce-scatter.2.cloned.1.call-done), calls=%async_computation.3 | async-start | bytes 524288 | tf_op jit(solution)/shard_map/all_to_all | solution.py:253
Sparse Core Ops, SparseCore 0:
  9.5 43.3 all-gather.4
  62.4 21.2 all-gather.8
  104.7 14.7 all-gather.6
  124.9 24.7 reduce-scatter.1
